TPU v7x, 32 devices: a whole 2x2x4 slice. The times are simulated.
32 devices in a mesh: grp: 2 (over x), tp: 16 (over z, y, core).
Axes of the slice: x: 2, y: 2, z: 4, core: 2. Of those that a mesh axis runs over, the one named last changes fastest.
Arguments:
- stream_in: bfloat16 [64, 4, 4096], P('grp'), parts along dimension 0, may hold values from -6 to 6
- state_in: float32 [2, 64, 8, 256, 256], P(None, 'grp', None, 'tp'), parts along dimension 1, may hold values from -0.8 to 0.8
- norm_gain: bfloat16 [2, 4096], replicated, may hold values from 0.099609375 to 1.8984375
- query_weight: bfloat16 [2, 4096, 2048], P(None, None, 'tp'), may hold values from -0.09375 to 0.09375
- key_weight: bfloat16 [2, 4096, 2048], P(None, None, 'tp'), may hold values from -0.09375 to 0.09375
- value_weight: bfloat16 [2, 4096, 8, 256], P(None, None, None, 'tp'), as said below
- gate_weight: bfloat16 [2, 4096, 8, 256], P(None, None, None, 'tp'), may hold values from -0.09375 to 0.09375
- group_gain: bfloat16 [2, 8, 256], P(None, None, 'tp'), may hold values from 0.099609375 to 1.8984375
- output_weight: bfloat16 [2, 8, 256, 4096], P(None, None, 'tp'), may hold values from -0.375 to 0.375
Outputs:
- stream_out: bfloat16 [64, 4, 4096], P('grp', None, 'tp'), parts along dimension 0
- state_out: float32 [2, 64, 8, 256, 256], P(None, 'grp', None, 'tp'), parts along dimension 1
There are 2 independent parts, one for each index of `grp`. A program takes and returns all parts, laid end to end along the dimension named above; an argument that names none is the same for every part. Nothing has to cross between parts.
Inputs may be any that keep to these rules, and one draw needn't show every extreme that they name: `value_weight`: real values; column scales of the value projection differ.
All inputs are finite; a program needn't handle non-finite values.
Results may differ from a plain program's by a relative error of at most 0.024.
Values may be sent and summed in bfloat16 or wider, within the bound.
No kernel may reach another device: no remote copies, remote signals or barrier semaphores. Data moves between devices by JAX's collectives and lax.ppermute only.
A program may use at most 64 MiB of HBM per device.

v0:
```python
import jax
import jax.numpy as jnp
from jax import lax
from jax.sharding import PartitionSpec as P

HEAD_DIM = 256
PAST = 1024
EPS_RMS = 1e-06
EPS_GROUP = 1e-05
ROTARY_BASE = 10000.0


def log_decays(count):
    return jnp.log(1.0 - jnp.power(2.0, -5.0 - jnp.arange(count, dtype=jnp.float32)))


def decay_tables(log_gamma, count):
    steps = jnp.arange(count, dtype=jnp.float32)
    gap = steps[:, None] - steps[None, :]
    intra = jnp.where(
        gap[None] >= 0, jnp.exp(log_gamma[:, None, None] * jnp.maximum(gap, 0.0)[None]), 0.0
    )
    q_decay = jnp.exp(log_gamma[None, :] * (steps[:, None] + 1.0))
    k_decay = jnp.exp(log_gamma[None, :] * (count - 1.0 - steps[:, None]))
    block_decay = jnp.exp(log_gamma * count)
    return (intra, q_decay, k_decay, block_decay)


def rotate(values, offset):
    half_dim = values.shape[-1] // 2
    freqs = jnp.power(
        ROTARY_BASE, -jnp.arange(half_dim, dtype=jnp.float32) * (2.0 / values.shape[-1])
    )
    places = (offset + jnp.arange(values.shape[1])).astype(jnp.float32)
    angles = places[:, None] * freqs[None, :]
    cosine = jnp.cos(angles)[None, :, None, :]
    sine = jnp.sin(angles)[None, :, None, :]
    first = values[..., :half_dim]
    second = values[..., half_dim:]
    return jnp.concatenate(
        [first * cosine - second * sine, second * cosine + first * sine], axis=-1
    )


def local(
    stream_in,
    state_in,
    norm_gain,
    query_weight,
    key_weight,
    value_weight,
    gate_weight,
    group_gain,
    output_weight,
):
    seqs, new_tok, width = stream_in.shape
    heads, local_dim = (value_weight.shape[2], value_weight.shape[3])
    head_dim = HEAD_DIM
    log_gamma = log_decays(heads)
    intra, q_decay, k_decay, block_decay = decay_tables(log_gamma, new_tok)
    highest = lax.Precision.HIGHEST
    share_cols = width // lax.axis_size("tp")
    col_start = lax.axis_index("tp") * share_cols
    layers = state_in.shape[0]
    stream = stream_in
    stream_share = stream_in
    new_states = []
    for layer_no in range(layers):
        stream_f = stream.astype(jnp.float32)
        normed = stream_f * lax.rsqrt(
            jnp.mean(stream_f * stream_f, axis=-1, keepdims=True) + EPS_RMS
        )
        normed = (normed * norm_gain[layer_no].astype(jnp.float32)).astype(jnp.bfloat16)
        flat = normed.reshape(seqs * new_tok, width)
        query_part = jnp.dot(flat, query_weight[layer_no], preferred_element_type=jnp.float32)
        query_part = query_part.astype(jnp.bfloat16).reshape(seqs, new_tok, -1)
        key_part = jnp.dot(flat, key_weight[layer_no], preferred_element_type=jnp.float32)
        key_part = key_part.astype(jnp.bfloat16).reshape(seqs, new_tok, -1)

        def project_local(weight):
            result = jnp.dot(
                flat, weight.reshape(width, heads * local_dim), preferred_element_type=jnp.float32
            )
            result = lax.optimization_barrier(result.astype(jnp.bfloat16))
            return result.astype(jnp.float32).reshape(seqs, new_tok, heads, local_dim)

        values_f = project_local(value_weight[layer_no])
        gates_f = project_local(gate_weight[layer_no])
        queries, key_rows = (
            lax.all_gather(query_part, "tp", axis=2, tiled=True),
            lax.all_gather(key_part, "tp", axis=2, tiled=True),
        )
        queries = queries.astype(jnp.float32).reshape(seqs, new_tok, heads, head_dim)
        key_rows = key_rows.astype(jnp.float32).reshape(seqs, new_tok, heads, head_dim)
        rot_q = rotate(queries, PAST)
        rot_k = rotate(key_rows, PAST) * head_dim ** (-0.5)
        scores = jnp.einsum("bthd,bshd->bhts", rot_q, rot_k, precision=highest) * intra[None]
        inner = jnp.einsum("bhts,bshe->bthe", scores, values_f, precision=highest)
        state = state_in[layer_no]
        carried = (
            jnp.einsum("bthd,bhed->bthe", rot_q, state, precision=highest)
            * q_decay[None, :, :, None]
        )
        mixed = inner + carried
        new_state = state * block_decay[None, :, None, None] + jnp.einsum(
            "bthe,bthd->bhed", values_f, rot_k * k_decay[None, :, :, None], precision=highest
        )
        new_states.append(new_state)
        totals, squares = lax.psum((jnp.sum(mixed, axis=-1), jnp.sum(mixed * mixed, axis=-1)), "tp")
        mean_o = (totals / head_dim)[..., None]
        var_o = (squares / head_dim)[..., None] - mean_o * mean_o
        normal = (
            (mixed - mean_o)
            * lax.rsqrt(var_o + EPS_GROUP)
            * group_gain[layer_no].astype(jnp.float32)[None, None]
        )
        gated = (jax.nn.silu(gates_f) * normal).astype(jnp.bfloat16)
        partial_out = jnp.dot(
            gated.reshape(seqs * new_tok, heads * local_dim),
            output_weight[layer_no].reshape(heads * local_dim, width),
            preferred_element_type=jnp.float32,
        ).reshape(seqs, new_tok, width)
        share_out = lax.psum_scatter(partial_out, "tp", scatter_dimension=2, tiled=True)
        own_cols = lax.dynamic_slice_in_dim(stream, col_start, share_cols, 2)
        stream_share = (own_cols.astype(jnp.float32) + share_out).astype(jnp.bfloat16)
        if layer_no + 1 < layers:
            stream = lax.all_gather(stream_share, "tp", axis=2, tiled=True)
    result = stream_share
    return (result, jnp.stack(new_states))


def solution(mesh):
    in_specs = (
        P("grp", None, None),
        P(None, "grp", None, "tp", None),
        P(),
        P(None, None, "tp"),
        P(None, None, "tp"),
        P(None, None, None, "tp"),
        P(None, None, None, "tp"),
        P(None, None, "tp"),
        P(None, None, "tp", None),
    )
    out_specs = (P("grp", None, "tp"), P(None, "grp", None, "tp", None))
    return jax.shard_map(local, mesh=mesh, in_specs=in_specs, out_specs=out_specs, check_vma=False)
```

profile of v0, /device:TPU:0, one launch (start us, length us, event | category | flops | bytes accessed | tf_op | source)
XLA Modules:
  0.0 433.5 jit_solution(2907268632619906550)
XLA Ops:
  7.3 0.7 bitcast_convert_fusion
  8.0 1.8 fusion.10
  9.9 0.8 slice_convert_fusion
  10.7 1.9 fusion.12
  12.9 1.8 convolution_convert_fusion.4
  14.8 0.4 convolution_convert_fusion.5
  15.2 24.6 %all_gather.15 = bf16[32,4,2048]{2,1,0:T(4,128)(2,1)S(1)} all-gather(bf16[32,4,128]{2,1,0:T(4,128)(2,1)S(1)} %bitcast.115), channel_id=1, replica_groups=mesh['grp'=2,'tp'=16] {'tp'}, dimensions={2}, use_global_device_ids=true | all-gather | bytes 557056 | tf_op jit(solution)/shard_map/all_gather | solution.py:90
  39.8 19.0 %all_gather.16 = bf16[32,4,2048]{2,1,0:T(4,128)(2,1)S(1)} all-gather(bf16[32,4,128]{2,1,0:T(4,128)(2,1)S(1)} %bitcast.114), channel_id=1, replica_groups=mesh['grp'=2,'tp'=16] {'tp'}, dimensions={2}, use_global_device_ids=true | all-gather | bytes 557056 | tf_op jit(solution)/shard_map/all_gather | solution.py:91
  59.3 0.6 multiply_subtract_fusion.2
  59.9 6.9 %fusion.4 = f32[32,8,4,16]{3,2,1,0:T(4,128)} fusion(f32[2,32,8,16,256]{4,3,2,1,0:T(8,128)} %param.10, f32[32,4,8,128]{3,1,2,0:T(4,128)S(1)} %get-tuple-element.46, f32[32,4,8,128]{3,1,2,0:T(4,128)S(1)} %get-tuple-element.47), kind=kOutput, calls=%fused_computation.7 | convolution fusion | flops 50593792 | bytes 5308416 | tf_op jit(solution)/shard_map/bthd,bhed->bthe/dot_general | solution.py:101
  66.8 2.0 copy.76
  68.9 2.7 fusion.56
  71.5 0.4 convolution_convert_fusion.6
  72.3 2.3 convolution_multiply_fusion.1
  74.6 1.0 fusion.38
  75.9 2.7 fusion.55
  78.7 0.4 convolution_convert_fusion.7
  79.6 1.8 fusion.54
  81.6 59.1 %all-reduce.1 = (f32[32,4,8]{0,2,1:T(8,128)S(1)}, f32[32,4,8]{0,2,1:T(8,128)S(1)}) all-reduce(f32[32,4,8]{0,2,1:T(8,128)S(1)} %get-tuple-element.15, f32[32,4,8]{0,2,1:T(8,128)S(1)} %get-tuple-element.14), channel_id=1, replica_groups=mesh['grp'=2,'tp'=16] {'tp'}, use_global_device_ids=true, to_apply=%region_4.5 | all-reduce | flops 2048 | bytes 16384 | tf_op jit(solution)/shard_map/psum | solution.py:109
  140.9 1.8 fusion.57
  142.8 0.9 constant_dynamic-slice_fusion
  143.6 58.3 %reduce-scatter.3.cloned.1.call-done = f32[32,4,256]{2,0,1:T(8,128)} async-done(((f32[32,4,4096]{2,0,1:T(8,128)}), f32[32,4,256]{2,0,1:T(8,128)}) %reduce-scatter.3.cloned.1.call-update) | async-done | bytes 131088 | tf_op jit(solution)/shard_map/reduce_scatter | solution.py:123
  201.9 1.5 add_convert_fusion.1
  203.8 36.5 %all-gather.2.cloned.1.call-done = bf16[32,4,4096]{2,0,1:T(8,128)(2,1)} async-done(((bf16[32,4,256]{2,0,1:T(8,128)(2,1)}), bf16[32,4,4096]{2,0,1:T(8,128)(2,1)}) %all-gather.2.cloned.1.call-update) | async-done | bytes 1048592 | tf_op jit(solution)/shard_map/all_gather | solution.py:127
  240.3 1.5 fusion.13
  241.8 1.5 fusion.15
  243.4 0.8 copy.78
  244.5 1.7 convolution_convert_fusion
  246.2 1.7 convolution_convert_fusion.1
  248.0 0.4 convolution_convert_fusion.2
  248.4 0.4 convolution_convert_fusion.3
  249.1 21.5 %all_gather.19 = bf16[32,4,2048]{2,1,0:T(4,128)(2,1)S(1)} all-gather(bf16[32,4,128]{2,1,0:T(4,128)(2,1)S(1)} %bitcast.113), channel_id=1, replica_groups=mesh['grp'=2,'tp'=16] {'tp'}, dimensions={2}, use_global_device_ids=true | all-gather | bytes 557056 | tf_op jit(solution)/shard_map/all_gather | solution.py:91
  270.6 18.9 %all_gather.18 = bf16[32,4,2048]{2,1,0:T(4,128)(2,1)S(1)} all-gather(bf16[32,4,128]{2,1,0:T(4,128)(2,1)S(1)} %bitcast.112), channel_id=1, replica_groups=mesh['grp'=2,'tp'=16] {'tp'}, dimensions={2}, use_global_device_ids=true | all-gather | bytes 557056 | tf_op jit(solution)/shard_map/all_gather | solution.py:90
  289.6 1.0 copy.80
  291.0 0.5 multiply_subtract_fusion
  291.4 0.8 copy-done.8
  292.2 6.6 %fusion = f32[32,8,4,16]{3,2,1,0:T(4,128)} fusion(f32[2,32,8,16,256]{4,3,2,1,0:T(8,128)} %param.10, f32[32,4,8,128]{3,1,2,0:T(4,128)S(1)} %get-tuple-element.44, f32[32,4,8,128]{3,1,2,0:T(4,128)S(1)} %get-tuple-element.45), kind=kOutput, calls=%fused_computation.2 | convolution fusion | flops 50593792 | bytes 5308416 | tf_op jit(solution)/shard_map/bthd,bhed->bthe/dot_general | solution.py:101
  298.8 1.3 copy.83
  300.1 3.4 convolution_multiply_fusion
  303.5 1.0 fusion.35
  305.0 59.2 %all-reduce = (f32[32,4,8]{0,2,1:T(8,128)S(1)}, f32[32,4,8]{0,2,1:T(8,128)S(1)}) all-reduce(f32[32,4,8]{0,2,1:T(8,128)S(1)} %get-tuple-element.13, f32[32,4,8]{0,2,1:T(8,128)S(1)} %get-tuple-element.12), channel_id=1, replica_groups=mesh['grp'=2,'tp'=16] {'tp'}, use_global_device_ids=true, to_apply=%region_10.11 | all-reduce | flops 2048 | bytes 16384 | tf_op jit(solution)/shard_map/psum | solution.py:109
  364.4 1.8 fusion.58
  366.3 4.5 %fusion.7 = f32[1,32,8,16,256]{4,3,2,1,0:T(8,128)S(1)} fusion(f32[2,32,8,16,256]{4,3,2,1,0:T(8,128)} %param.10, f32[8]{0:T(128)S(1)} %multiply_exponential_fusion.1, f32[32,4,8,128]{3,1,2,0:T(4,128)S(1)} %copy-done.5, f32[32,4,8,128]{3,1,2,0:T(4,128)S(1)} %copy-done.3, f32[4,8]{0,1:T(8,128)S(1)} %copy.85, bf16[32,4,8,16]{3,2,1,0:T(8,128)(2,1)S(1)} %reshape.319), kind=kOutput, calls=%fused_computation.10 | convolution fusion | flops 52953088 | bytes 9470112 | tf_op jit(solution)/shard_map/bthe,bthd->bhed/dot_general | solution.py:105
  370.8 4.5 %fusion.3 = f32[1,32,8,16,256]{4,3,2,1,0:T(8,128)S(1)} fusion(f32[2,32,8,16,256]{4,3,2,1,0:T(8,128)} %param.10, f32[8]{0:T(128)S(1)} %multiply_exponential_fusion.1, f32[32,4,8,128]{3,1,2,0:T(4,128)S(1)} %copy-done.7, f32[32,4,8,128]{3,1,2,0:T(4,128)S(1)} %get-tuple-element.28, f32[4,8]{0,1:T(8,128)S(1)} %copy.85, bf16[32,4,8,16]{3,2,1,0:T(8,128)(2,1)S(1)} %reshape.329), kind=kOutput, calls=%fused_computation.5 | convolution fusion | flops 52953088 | bytes 9470112 | tf_op jit(solution)/shard_map/bthe,bthd->bhed/dot_general | solution.py:105
  375.3 4.4 %pad_maximum_fusion = f32[2,32,8,16,256]{4,3,2,1,0:T(8,128)} fusion(f32[1,32,8,16,256]{4,3,2,1,0:T(8,128)S(1)} %fusion.3, f32[1,32,8,16,256]{4,3,2,1,0:T(8,128)S(1)} %fusion.7), kind=kLoop, calls=%fused_computation | loop fusion | flops 2097152 | bytes 16777216 | tf_op jit(solution)/shard_map/stack | solution.py:129
  379.8 45.6 %reduce-scatter.5.cloned.1.call-done = f32[32,4,256]{2,0,1:T(8,128)} async-done(((f32[32,4,4096]{2,0,1:T(8,128)}), f32[32,4,256]{2,0,1:T(8,128)}) %reduce-scatter.5.cloned.1.call-update) | async-done | bytes 131088 | tf_op jit(solution)/shard_map/reduce_scatter | solution.py:123
  425.4 0.9 add_convert_fusion
  426.3 0.7 copy.88
  (61 shorter events, 4.5 us)
Async XLA Ops:
  7.2 194.8 %reduce-scatter.3.cloned.1.call-start = ((), (), s32[]{:S(2)}) async-start(), calls=%async_computation.2 | async-start | bytes 2228224 | tf_op jit(solution)/shard_map/reduce_scatter | solution.py:123
  12.9 1.9 copy-start.11
  59.9 12.4 %copy-start.2 = (f32[32,4,8,128]{3,1,2,0:T(4,128)}, f32[32,4,8,128]{3,1,2,0:T(4,128)S(1)}, u32[]{:S(2)}) copy-start(f32[32,4,8,128]{3,1,2,0:T(4,128)S(1)} %get-tuple-element.32) | copy-start | bytes 1572868
  59.9 12.4 %copy-start.4 = (f32[32,4,8,128]{3,1,2,0:T(4,128)}, f32[32,4,8,128]{3,1,2,0:T(4,128)S(1)}, u32[]{:S(2)}) copy-start(f32[32,4,8,128]{3,1,2,0:T(4,128)S(1)} %get-tuple-element.33) | copy-start | bytes 1572868
  79.6 1.9 copy-start.9
  142.7 97.6 %all-gather.2.cloned.1.call-start = ((), (), s32[]{:S(2)}) async-start(), calls=%async_computation.3 | async-start | bytes 1114112 | tf_op jit(solution)/shard_map/all_gather | solution.py:127
  203.5 221.9 %reduce-scatter.5.cloned.1.call-start = ((), (), s32[]{:S(2)}) async-start(), calls=%async_computation.4 | async-start | bytes 2228224 | tf_op jit(solution)/shard_map/reduce_scatter | solution.py:123
  244.5 3.5 copy-start
  246.2 2.2 copy-start.1
  291.4 0.8 copy-start.8
  291.4 8.7 %copy-start.6 = (f32[32,4,8,128]{3,1,2,0:T(4,128)}, f32[32,4,8,128]{3,1,2,0:T(4,128)S(1)}, u32[]{:S(2)}) copy-start(f32[32,4,8,128]{3,1,2,0:T(4,128)S(1)} %get-tuple-element.29) | copy-start | bytes 1572868
  303.5 60.8 %copy-start.10 = (f32[32,4,8,16]{0,3,2,1:T(8,128)S(1)}, f32[32,4,8,16]{0,3,2,1:T(8,128)}, u32[]{:S(2)}) copy-start(f32[32,4,8,16]{0,3,2,1:T(8,128)} %copy.80) | copy-start | bytes 196612
  364.4 2.0 copy-start.3
  364.4 1.9 copy-start.5
  366.3 4.5 %copy-start.7 = (f32[32,4,8,128]{3,1,2,0:T(4,128)S(1)}, f32[32,4,8,128]{3,1,2,0:T(4,128)}, u32[]{:S(2)}) copy-start(f32[32,4,8,128]{3,1,2,0:T(4,128)} %copy-done.6) | copy-start | bytes 1572868
Sparse Core Ops, SparseCore 0:
  142.8 59.0 reduce-scatter.2
  204.7 35.5 all-gather.1
  366.3 58.9 reduce-scatter.4
where the time goes:
time: 434 us
  blocking collectives  202 us (47%)
  waiting for transfers between devices  140 us (32%)
  matrix products  41.1 us (9%)
  other arithmetic  17.9 us (4%)
  local copies, waits for them, and re-layouts  17.2 us (4%)
  between operations  14.2 us (3%)
    psum x2, blocking collectives, local(): lax.psum((jnp.sum(mixed, axis=-1), jnp.sum(mixed * mixed, axis=-1)), 'tp')  118 us
    reduce_scatter x2, waiting for transfers between devices, local(): lax.psum_scatter(partial_out, 'tp', scatter_dimension=2, tiled=True)  104 us
    all_gather x2, blocking collectives, local(): lax.all_gather(query_part, 'tp', axis=2, tiled=True)  43.5 us
    all_gather x2, blocking collectives, local(): lax.all_gather(key_part, 'tp', axis=2, tiled=True)  40.6 us
    all_gather x1, waiting for transfers between devices, local(): stream = lax.all_gather(stream_share, 'tp', axis=2, tiled=True)  36.5 us
    dot_general x2, matrix products, local(): jnp.einsum('bthd,bhed->bthe', rot_q, state, precision=highest)  13.5 us
    dot_general x2, matrix products, local(): jnp.einsum('bthe,bthd->bhed', values_f, rot_k * k_decay[None, :, :, None]...  8.98 us
  transfers between devices with their start and end apart: 3, of which 3 were waited for; matrix products, arithmetic and copies ran while one was open for 3% of the time, Pallas kernels for 0%

commit v1 on v0

--- a/solution.py
+++ b/solution.py
@@ -124,7 +124,24 @@
         own_cols = lax.dynamic_slice_in_dim(stream, col_start, share_cols, 2)
         stream_share = (own_cols.astype(jnp.float32) + share_out).astype(jnp.bfloat16)
         if layer_no + 1 < layers:
-            stream = lax.all_gather(stream_share, "tp", axis=2, tiled=True)
+            ways, here, step = (lax.axis_size("tp"), lax.axis_index("tp"), stream_share.shape[2])
+            shape = [n * ways if d == 2 else n for d, n in enumerate(stream_share.shape)]
+            stream = lax.dynamic_update_slice_in_dim(
+                jnp.zeros(shape, stream_share.dtype), stream_share, here * step, axis=2
+            )
+            going_up = going_down = stream_share
+            for far in range(1, ways // 2 + 1):
+                going_up = lax.ppermute(going_up, "tp", [(d, (d + 1) % ways) for d in range(ways)])
+                stream = lax.dynamic_update_slice_in_dim(
+                    stream, going_up, (here - far) % ways * step, axis=2
+                )
+                if 2 * far < ways:
+                    going_down = lax.ppermute(
+                        going_down, "tp", [(d, (d - 1) % ways) for d in range(ways)]
+                    )
+                    stream = lax.dynamic_update_slice_in_dim(
+                        stream, going_down, (here + far) % ways * step, axis=2
+                    )
     result = stream_share
     return (result, jnp.stack(new_states))
 

time: 434 us -> 455 us (1.048)
  starting transfers between devices: 0.34 us -> 31.4 us
  waiting for transfers between devices: 140 us -> 123 us
  local copies, waits for them, and re-layouts: 17.2 us -> 23.2 us
    all_gather x1 -> x0, waiting for transfers between devices: 36.5 us -> none  [local(): stream = lax.all_gather(stream_share, 'tp', axis=2, tiled=True)]
    ppermute x0 -> x15, starting transfers between devices: none -> 31.3 us  [the longest x7 31.3 us: local(): lax.ppermute(going_down, 'tp', [(d, (d - 1) % ways) for d in range(ways)])]
    ppermute x0 -> x15, waiting for transfers between devices: none -> 19.7 us  [the longest x8 19.6 us: local(): lax.ppermute(going_up, 'tp', [(d, (d + 1) % ways) for d in range(ways)])]
  transfers between devices with their start and end apart: 3 -> 17, of which waited for: 3 -> 10; matrix products, arithmetic and copies ran while one was open for 3% -> 3% of each run, Pallas kernels for 0% -> 0%
where the time goes in v1:
time: 455 us; the launch traced here: 454 us
  blocking collectives  202 us (44%)
  waiting for transfers between devices  123 us (27%)
  matrix products  41.5 us (9%)
  starting transfers between devices  31.4 us (7%)
  local copies, waits for them, and re-layouts  23.2 us (5%)
  other arithmetic  19.2 us (4%)
  between operations  14.6 us (3%)
    psum x2, blocking collectives, local(): lax.psum((jnp.sum(mixed, axis=-1), jnp.sum(mixed * mixed, axis=-1)), 'tp')  117 us
    reduce_scatter x2, waiting for transfers between devices, local(): lax.psum_scatter(partial_out, 'tp', scatter_dimension=2, tiled=True)  103 us
    all_gather x2, blocking collectives, local(): lax.all_gather(query_part, 'tp', axis=2, tiled=True)  47 us
    all_gather x2, blocking collectives, local(): lax.all_gather(key_part, 'tp', axis=2, tiled=True)  37.7 us
    ppermute x7, starting transfers between devices, local(): lax.ppermute(going_down, 'tp', [(d, (d - 1) % ways) for d in range(ways)])  31.3 us
    ppermute x8, waiting for transfers between devices, local(): lax.ppermute(going_up, 'tp', [(d, (d + 1) % ways) for d in range(ways)])  19.6 us
    dot_general x2, matrix products, local(): jnp.einsum('bthd,bhed->bthe', rot_q, state, precision=highest)  13.5 us
  transfers between devices with their start and end apart: 17, of which 10 were waited for; matrix products, arithmetic and copies ran while one was open for 3% of the time, Pallas kernels for 0%

profile of v1, /device:TPU:0, one launch (start us, length us, event | category | flops | bytes accessed | tf_op | source)
XLA Modules:
  0.0 454.2 jit_solution(17469151971419795445)
XLA Ops:
  8.0 1.8 fusion.10
  10.7 2.0 fusion.12
  13.0 1.8 convolution_convert_fusion.4
  15.3 24.6 %all_gather.12 = bf16[32,4,2048]{2,1,0:T(4,128)(2,1)S(1)} all-gather(bf16[32,4,128]{2,1,0:T(4,128)(2,1)S(1)} %bitcast.115), channel_id=1, replica_groups=mesh['grp'=2,'tp'=16] {'tp'}, dimensions={2}, use_global_device_ids=true | all-gather | bytes 557056 | tf_op jit(solution)/shard_map/all_gather | solution.py:90
  39.9 19.0 %all_gather.13 = bf16[32,4,2048]{2,1,0:T(4,128)(2,1)S(1)} all-gather(bf16[32,4,128]{2,1,0:T(4,128)(2,1)S(1)} %bitcast.114), channel_id=1, replica_groups=mesh['grp'=2,'tp'=16] {'tp'}, dimensions={2}, use_global_device_ids=true | all-gather | bytes 557056 | tf_op jit(solution)/shard_map/all_gather | solution.py:91
  60.0 6.9 %fusion.4 = f32[32,8,4,16]{3,2,1,0:T(4,128)} fusion(f32[2,32,8,16,256]{4,3,2,1,0:T(8,128)} %param.10, f32[32,4,8,128]{3,1,2,0:T(4,128)S(1)} %get-tuple-element.48, f32[32,4,8,128]{3,1,2,0:T(4,128)S(1)} %get-tuple-element.49), kind=kOutput, calls=%fused_computation.7 | convolution fusion | flops 50593792 | bytes 5308416 | tf_op jit(solution)/shard_map/bthd,bhed->bthe/dot_general | solution.py:101
  66.9 2.0 copy.76
  69.0 2.7 fusion.56
  72.4 2.3 convolution_multiply_fusion.1
  76.1 2.7 fusion.55
  79.7 1.8 fusion.54
  82.4 59.1 %all-reduce.1 = (f32[32,4,8]{0,2,1:T(8,128)S(1)}, f32[32,4,8]{0,2,1:T(8,128)S(1)}) all-reduce(f32[32,4,8]{0,2,1:T(8,128)S(1)} %get-tuple-element.15, f32[32,4,8]{0,2,1:T(8,128)S(1)} %get-tuple-element.14), channel_id=1, replica_groups=mesh['grp'=2,'tp'=16] {'tp'}, use_global_device_ids=true, to_apply=%region_4.5 | all-reduce | flops 2048 | bytes 16384 | tf_op jit(solution)/shard_map/psum | solution.py:109
  141.7 1.8 fusion.57
  144.4 58.3 %reduce-scatter.3.cloned.1.call-done = f32[32,4,256]{2,0,1:T(8,128)} async-done(((f32[32,4,4096]{2,0,1:T(8,128)}), f32[32,4,256]{2,0,1:T(8,128)}) %reduce-scatter.3.cloned.1.call-update) | async-done | bytes 131088 | tf_op jit(solution)/shard_map/reduce_scatter | solution.py:123
  203.7 4.4 collective-permute-start.1
  208.2 1.9 collective-permute-done
  210.1 4.4 collective-permute-start.3
  214.6 2.0 collective-permute-done.2
  216.6 4.4 collective-permute-start.5
  221.1 1.9 collective-permute-done.4
  223.0 4.5 collective-permute-start.7
  227.5 1.9 collective-permute-done.6
  229.4 4.5 collective-permute-start.9
  233.9 1.9 collective-permute-done.8
  235.8 4.5 collective-permute-start.11
  240.3 1.9 collective-permute-done.10
  242.2 4.5 collective-permute-start.13
  246.7 1.9 collective-permute-done.12
  248.6 6.3 %collective-permute-done.14 = bf16[32,4,256]{2,0,1:T(8,128)(2,1)S(1)} collective-permute-done((bf16[32,4,256]{2,0,1:T(8,128)(2,1)S(1)}, bf16[32,4,256]{2,0,1:T(8,128)(2,1)S(1)}, u32[]{:S(2)}, u32[]{:S(2)}) %collective-permute-start.14) | collective-permute-done | bytes 65568 | tf_op jit(solution)/shard_map/ppermute | solution.py:134
  255.6 1.8 copy.78
  257.4 1.3 reshape.326
  258.7 1.7 convolution_convert_fusion
  260.5 1.7 convolution_convert_fusion.1
  263.3 18.7 %all_gather.15 = bf16[32,4,2048]{2,1,0:T(4,128)(2,1)S(1)} all-gather(bf16[32,4,128]{2,1,0:T(4,128)(2,1)S(1)} %bitcast.113), channel_id=1, replica_groups=mesh['grp'=2,'tp'=16] {'tp'}, dimensions={2}, use_global_device_ids=true | all-gather | bytes 557056 | tf_op jit(solution)/shard_map/all_gather | solution.py:91
  282.0 22.4 %all_gather.14 = bf16[32,4,2048]{2,1,0:T(4,128)(2,1)} all-gather(bf16[32,4,128]{2,1,0:T(4,128)(2,1)S(1)} %bitcast.112), channel_id=1, replica_groups=mesh['grp'=2,'tp'=16] {'tp'}, dimensions={2}, use_global_device_ids=true | all-gather | bytes 557056 | tf_op jit(solution)/shard_map/all_gather | solution.py:90
  305.4 2.0 copy.80
  307.5 1.2 convert.12
  308.8 1.2 multiply_subtract_fusion
  311.0 6.6 %fusion = f32[32,8,4,16]{3,2,1,0:T(4,128)} fusion(f32[2,32,8,16,256]{4,3,2,1,0:T(8,128)} %param.10, f32[32,4,8,128]{3,1,2,0:T(4,128)S(1)} %get-tuple-element.46, f32[32,4,8,128]{3,1,2,0:T(4,128)S(1)} %get-tuple-element.47), kind=kOutput, calls=%fused_computation.2 | convolution fusion | flops 50593792 | bytes 5308416 | tf_op jit(solution)/shard_map/bthd,bhed->bthe/dot_general | solution.py:101
  317.6 1.3 copy.83
  318.9 3.7 convolution_multiply_fusion
  324.6 1.1 fusion.50
  325.8 57.9 %all-reduce = (f32[32,4,8]{0,2,1:T(8,128)S(1)}, f32[32,4,8]{0,2,1:T(8,128)S(1)}) all-reduce(f32[32,4,8]{0,2,1:T(8,128)S(1)} %get-tuple-element.13, f32[32,4,8]{0,2,1:T(8,128)S(1)} %get-tuple-element.12), channel_id=1, replica_groups=mesh['grp'=2,'tp'=16] {'tp'}, use_global_device_ids=true, to_apply=%region_10.11 | all-reduce | flops 2048 | bytes 16384 | tf_op jit(solution)/shard_map/psum | solution.py:109
  384.8 1.8 fusion.58
  387.6 4.5 fusion.7
  392.2 4.5 fusion.3
  396.7 4.4 pad_maximum_fusion
  401.1 44.6 %reduce-scatter.5.cloned.1.call-done = f32[32,4,256]{2,0,1:T(8,128)} async-done(((f32[32,4,4096]{2,0,1:T(8,128)}), f32[32,4,256]{2,0,1:T(8,128)}) %reduce-scatter.5.cloned.1.call-update) | async-done | bytes 131088 | tf_op jit(solution)/shard_map/reduce_scatter | solution.py:123
  (112 shorter events, 19.2 us)
Async XLA Ops:
  7.2 195.5 %reduce-scatter.3.cloned.1.call-start = ((), (), s32[]{:S(2)}) async-start(), calls=%async_computation.2 | async-start | bytes 2228224 | tf_op jit(solution)/shard_map/reduce_scatter | solution.py:123
  13.0 1.9 copy-start.15
  60.0 12.4 %copy-start.2 = (f32[32,4,8,128]{3,1,2,0:T(4,128)}, f32[32,4,8,128]{3,1,2,0:T(4,128)S(1)}, u32[]{:S(2)}) copy-start(f32[32,4,8,128]{3,1,2,0:T(4,128)S(1)} %get-tuple-element.34) | copy-start | bytes 1572868
  60.0 12.4 %copy-start.4 = (f32[32,4,8,128]{3,1,2,0:T(4,128)}, f32[32,4,8,128]{3,1,2,0:T(4,128)S(1)}, u32[]{:S(2)}) copy-start(f32[32,4,8,128]{3,1,2,0:T(4,128)S(1)} %get-tuple-element.35) | copy-start | bytes 1572868
  72.4 2.3 copy-start.12
  79.7 2.5 copy-start.11
  143.5 302.3 %reduce-scatter.5.cloned.1.call-start = ((), (), s32[]{:S(2)}) async-start(), calls=%async_computation.3 | async-start | bytes 2228224 | tf_op jit(solution)/shard_map/reduce_scatter | solution.py:123
  203.7 6.4 %collective-permute-start = (bf16[32,4,256]{2,0,1:T(8,128)(2,1)S(1)}, bf16[32,4,256]{2,0,1:T(8,128)(2,1)S(1)}, u32[]{:S(2)}, u32[]{:S(2)}) collective-permute-start(bf16[32,4,256]{2,0,1:T(8,128)(2,1)S(1)} %get-tuple-element.22), channel_id=1, source_target_pairs={{0,1},{1,2},{2,3},{3,4},{4,5},{5,6},{6,7},{7,8},{8,9},{9,10},{10,1... | collective-permute-start | bytes 196616 | tf_op jit(solution)/shard_map/ppermute | solution.py:134
  203.7 6.4 %collective-permute-start.1 = (bf16[32,4,256]{2,0,1:T(8,128)(2,1)S(1)}, bf16[32,4,256]{2,0,1:T(8,128)(2,1)S(1)}, u32[]{:S(2)}, u32[]{:S(2)}) collective-permute-start(bf16[32,4,256]{2,0,1:T(8,128)(2,1)S(1)} %get-tuple-element.22), channel_id=1, source_target_pairs={{0,15},{1,0},{2,1},{3,2},{4,3},{5,4},{6,5},{7,6},{8,7},{9,8},{10,9... | collective-permute-start | bytes 196616 | tf_op jit(solution)/shard_map/ppermute | solution.py:139
  210.1 6.5 %collective-permute-start.2 = (bf16[32,4,256]{2,0,1:T(8,128)(2,1)S(1)}, bf16[32,4,256]{2,0,1:T(8,128)(2,1)S(1)}, u32[]{:S(2)}, u32[]{:S(2)}) collective-permute-start(bf16[32,4,256]{2,0,1:T(8,128)(2,1)S(1)} %collective-permute-done), channel_id=1, source_target_pairs={{0,1},{1,2},{2,3},{3,4},{4,5},{5,6},{6,7},{7,8},{8,9},{9,10},{10,1... | collective-permute-start | bytes 196616 | tf_op jit(solution)/shard_map/ppermute | solution.py:134
  210.1 6.5 %collective-permute-start.3 = (bf16[32,4,256]{2,0,1:T(8,128)(2,1)S(1)}, bf16[32,4,256]{2,0,1:T(8,128)(2,1)S(1)}, u32[]{:S(2)}, u32[]{:S(2)}) collective-permute-start(bf16[32,4,256]{2,0,1:T(8,128)(2,1)S(1)} %collective-permute-done.1), channel_id=1, source_target_pairs={{0,15},{1,0},{2,1},{3,2},{4,3},{5,4},{6,5},{7,6},{8,7},{9,8},{10,9... | collective-permute-start | bytes 196616 | tf_op jit(solution)/shard_map/ppermute | solution.py:139
  216.6 6.4 %collective-permute-start.4 = (bf16[32,4,256]{2,0,1:T(8,128)(2,1)S(1)}, bf16[32,4,256]{2,0,1:T(8,128)(2,1)S(1)}, u32[]{:S(2)}, u32[]{:S(2)}) collective-permute-start(bf16[32,4,256]{2,0,1:T(8,128)(2,1)S(1)} %collective-permute-done.2), channel_id=1, source_target_pairs={{0,1},{1,2},{2,3},{3,4},{4,5},{5,6},{6,7},{7,8},{8,9},{9,10},{10,1... | collective-permute-start | bytes 196616 | tf_op jit(solution)/shard_map/ppermute | solution.py:134
  216.6 6.4 %collective-permute-start.5 = (bf16[32,4,256]{2,0,1:T(8,128)(2,1)S(1)}, bf16[32,4,256]{2,0,1:T(8,128)(2,1)S(1)}, u32[]{:S(2)}, u32[]{:S(2)}) collective-permute-start(bf16[32,4,256]{2,0,1:T(8,128)(2,1)S(1)} %collective-permute-done.3), channel_id=1, source_target_pairs={{0,15},{1,0},{2,1},{3,2},{4,3},{5,4},{6,5},{7,6},{8,7},{9,8},{10,9... | collective-permute-start | bytes 196616 | tf_op jit(solution)/shard_map/ppermute | solution.py:139
  223.0 6.4 %collective-permute-start.6 = (bf16[32,4,256]{2,0,1:T(8,128)(2,1)S(1)}, bf16[32,4,256]{2,0,1:T(8,128)(2,1)S(1)}, u32[]{:S(2)}, u32[]{:S(2)}) collective-permute-start(bf16[32,4,256]{2,0,1:T(8,128)(2,1)S(1)} %collective-permute-done.4), channel_id=1, source_target_pairs={{0,1},{1,2},{2,3},{3,4},{4,5},{5,6},{6,7},{7,8},{8,9},{9,10},{10,1... | collective-permute-start | bytes 196616 | tf_op jit(solution)/shard_map/ppermute | solution.py:134
  223.0 6.4 %collective-permute-start.7 = (bf16[32,4,256]{2,0,1:T(8,128)(2,1)S(1)}, bf16[32,4,256]{2,0,1:T(8,128)(2,1)S(1)}, u32[]{:S(2)}, u32[]{:S(2)}) collective-permute-start(bf16[32,4,256]{2,0,1:T(8,128)(2,1)S(1)} %collective-permute-done.5), channel_id=1, source_target_pairs={{0,15},{1,0},{2,1},{3,2},{4,3},{5,4},{6,5},{7,6},{8,7},{9,8},{10,9... | collective-permute-start | bytes 196616 | tf_op jit(solution)/shard_map/ppermute | solution.py:139
  229.4 6.4 %collective-permute-start.8 = (bf16[32,4,256]{2,0,1:T(8,128)(2,1)S(1)}, bf16[32,4,256]{2,0,1:T(8,128)(2,1)S(1)}, u32[]{:S(2)}, u32[]{:S(2)}) collective-permute-start(bf16[32,4,256]{2,0,1:T(8,128)(2,1)S(1)} %collective-permute-done.6), channel_id=1, source_target_pairs={{0,1},{1,2},{2,3},{3,4},{4,5},{5,6},{6,7},{7,8},{8,9},{9,10},{10,1... | collective-permute-start | bytes 196616 | tf_op jit(solution)/shard_map/ppermute | solution.py:134
  229.4 6.4 %collective-permute-start.9 = (bf16[32,4,256]{2,0,1:T(8,128)(2,1)S(1)}, bf16[32,4,256]{2,0,1:T(8,128)(2,1)S(1)}, u32[]{:S(2)}, u32[]{:S(2)}) collective-permute-start(bf16[32,4,256]{2,0,1:T(8,128)(2,1)S(1)} %collective-permute-done.7), channel_id=1, source_target_pairs={{0,15},{1,0},{2,1},{3,2},{4,3},{5,4},{6,5},{7,6},{8,7},{9,8},{10,9... | collective-permute-start | bytes 196616 | tf_op jit(solution)/shard_map/ppermute | solution.py:139
  235.8 6.4 %collective-permute-start.10 = (bf16[32,4,256]{2,0,1:T(8,128)(2,1)S(1)}, bf16[32,4,256]{2,0,1:T(8,128)(2,1)S(1)}, u32[]{:S(2)}, u32[]{:S(2)}) collective-permute-start(bf16[32,4,256]{2,0,1:T(8,128)(2,1)S(1)} %collective-permute-done.8), channel_id=1, source_target_pairs={{0,1},{1,2},{2,3},{3,4},{4,5},{5,6},{6,7},{7,8},{8,9},{9,10},{10,1... | collective-permute-start | bytes 196616 | tf_op jit(solution)/shard_map/ppermute | solution.py:134
  235.8 6.4 %collective-permute-start.11 = (bf16[32,4,256]{2,0,1:T(8,128)(2,1)S(1)}, bf16[32,4,256]{2,0,1:T(8,128)(2,1)S(1)}, u32[]{:S(2)}, u32[]{:S(2)}) collective-permute-start(bf16[32,4,256]{2,0,1:T(8,128)(2,1)S(1)} %collective-permute-done.9), channel_id=1, source_target_pairs={{0,15},{1,0},{2,1},{3,2},{4,3},{5,4},{6,5},{7,6},{8,7},{9,8},{10,9... | collective-permute-start | bytes 196616 | tf_op jit(solution)/shard_map/ppermute | solution.py:139
  242.2 6.4 %collective-permute-start.12 = (bf16[32,4,256]{2,0,1:T(8,128)(2,1)S(1)}, bf16[32,4,256]{2,0,1:T(8,128)(2,1)S(1)}, u32[]{:S(2)}, u32[]{:S(2)}) collective-permute-start(bf16[32,4,256]{2,0,1:T(8,128)(2,1)S(1)} %collective-permute-done.10), channel_id=1, source_target_pairs={{0,1},{1,2},{2,3},{3,4},{4,5},{5,6},{6,7},{7,8},{8,9},{9,10},{10,1... | collective-permute-start | bytes 196616 | tf_op jit(solution)/shard_map/ppermute | solution.py:134
  242.2 6.4 %collective-permute-start.13 = (bf16[32,4,256]{2,0,1:T(8,128)(2,1)S(1)}, bf16[32,4,256]{2,0,1:T(8,128)(2,1)S(1)}, u32[]{:S(2)}, u32[]{:S(2)}) collective-permute-start(bf16[32,4,256]{2,0,1:T(8,128)(2,1)S(1)} %collective-permute-done.11), channel_id=1, source_target_pairs={{0,15},{1,0},{2,1},{3,2},{4,3},{5,4},{6,5},{7,6},{8,7},{9,8},{10,9... | collective-permute-start | bytes 196616 | tf_op jit(solution)/shard_map/ppermute | solution.py:139
  248.5 6.4 %collective-permute-start.14 = (bf16[32,4,256]{2,0,1:T(8,128)(2,1)S(1)}, bf16[32,4,256]{2,0,1:T(8,128)(2,1)S(1)}, u32[]{:S(2)}, u32[]{:S(2)}) collective-permute-start(bf16[32,4,256]{2,0,1:T(8,128)(2,1)S(1)} %collective-permute-done.12), channel_id=1, source_target_pairs={{0,1},{1,2},{2,3},{3,4},{4,5},{5,6},{6,7},{7,8},{8,9},{9,10},{10,1... | collective-permute-start | bytes 196616 | tf_op jit(solution)/shard_map/ppermute | solution.py:134
  258.7 3.5 copy-start
  260.5 2.2 copy-start.1
  310.0 0.8 copy-start.9
  310.0 1.0 copy-start.10
  310.0 8.9 %copy-start.6 = (f32[32,4,8,128]{3,1,2,0:T(4,128)}, f32[32,4,8,128]{3,1,2,0:T(4,128)S(1)}, u32[]{:S(2)}) copy-start(f32[32,4,8,128]{3,1,2,0:T(4,128)S(1)} %get-tuple-element.30) | copy-start | bytes 1572868
  311.0 7.9 %copy-start.13 = (f32[8,4,4]{2,1,0:T(4,128)S(1)}, f32[8,4,4]{2,1,0:T(4,128)}, u32[]{:S(2)}) copy-start(f32[8,4,4]{2,1,0:T(4,128)} %copy-done.12) | copy-start | bytes 1540
  384.8 1.8 copy-start.14
  384.8 1.9 copy-start.3
  386.6 1.0 copy-start.5
  387.6 4.5 copy-start.7
  387.6 4.5 copy-start.8
Sparse Core Ops, SparseCore 0:
  143.6 59.0 reduce-scatter.2
  386.7 58.9 reduce-scatter.4
